TPU v7x, 32 devices: a whole 2x2x4 slice. The times are simulated.
32 devices in a mesh: ep: 8 (over z, x), tp: 4 (over y, core).
Axes of the slice: x: 2, y: 2, z: 4, core: 2. Of those that a mesh axis runs over, the one named last changes fastest.
Arguments:
- tokens: bfloat16 [256, 4096], P('ep'), may hold values from -6 to 6
- routes: int32 [256, 4], P('ep'), may hold values from 0 to 7, all different within a row; in each aligned block of 32 rows (0 to 31, 32 to 63, ...) at most 24 rows name the same one
- mix_weights: float32 [256, 4], P('ep'), may hold values from 0.2 to 1
- pre_gain: float32 [4096], replicated, may hold values from 0.1 to 1.9
- gate_weight: bfloat16 [8, 4096, 2048], P('ep', None, 'tp'), may hold values from -0.09375 to 0.09375
- up_weight: bfloat16 [8, 4096, 2048], P('ep', None, 'tp'), may hold values from -0.09375 to 0.09375
- down_weight: bfloat16 [8, 2048, 4096], P('ep', 'tp'), may hold values from -1 to 1
- post_gain: float32 [4096], P('tp'), may hold values from 0.1 to 1.9
Outputs:
- layer_out: bfloat16 [256, 4096], P('ep', 'tp')
Inputs may be any that keep to these rules, and one draw needn't show every extreme that they name: `routes`: within a row the 4 experts differ; among the rows of one index of ep no expert is named more than 24 times.
All inputs are finite; a program needn't handle non-finite values.
Results may differ from a plain program's by a relative error of at most 0.019.
Values may be sent and summed in bfloat16 or wider, within the bound.
A program may use at most 64 MiB of HBM per device.

v0:
```python
import jax
import jax.numpy as jnp
from jax import lax
from jax.sharding import PartitionSpec as P

epsilon = 1e-06


def on_device(
    tokens, routes, mix_weights, pre_gain, gate_weight, up_weight, down_weight, post_gain
):
    tok_rows, width = tokens.shape
    top_count = routes.shape[1]
    experts = lax.axis_size("ep")
    capacity = min(tok_rows, max(2, (3 * tok_rows * top_count + 2 * experts - 1) // (2 * experts)))
    floats = tokens.astype(jnp.float32)
    normed = (
        floats * lax.rsqrt(jnp.mean(floats * floats, axis=-1, keepdims=True) + epsilon) * pre_gain
    ).astype(jnp.bfloat16)
    chosen = routes.reshape(-1)
    onehot = (chosen[:, None] == jnp.arange(experts, dtype=jnp.int32)[None, :]).astype(jnp.int32)
    before = jnp.cumsum(onehot, axis=0) - onehot
    slot_rank = jnp.sum(before * onehot, axis=1)
    target = chosen * capacity + slot_rank
    placed = target[:, None] == jnp.arange(experts * capacity, dtype=jnp.int32)[None, :]
    by_choice = placed.reshape(tok_rows, top_count, experts * capacity)
    picked = jnp.any(by_choice, axis=1).astype(jnp.bfloat16)
    outgoing = jnp.einsum("tc,td->cd", picked, normed, preferred_element_type=jnp.float32).astype(
        jnp.bfloat16
    )
    outgoing = outgoing.reshape(experts, capacity, width)
    slice_width = width // lax.axis_size("tp")
    outgoing_part = lax.dynamic_slice_in_dim(
        outgoing, lax.axis_index("tp") * slice_width, slice_width, 2
    )
    arrived = lax.all_to_all(outgoing_part, "ep", split_axis=0, concat_axis=0, tiled=True)
    arrived = lax.all_gather(arrived, "tp", axis=2, tiled=True)
    arrived_rows = arrived.reshape(experts * capacity, width)
    gate_act = jnp.dot(arrived_rows, gate_weight[0], preferred_element_type=jnp.float32)
    up_act = jnp.dot(arrived_rows, up_weight[0], preferred_element_type=jnp.float32)
    hidden = (jax.nn.silu(gate_act) * up_act).astype(jnp.bfloat16)
    partial_value = jnp.dot(hidden, down_weight[0], preferred_element_type=jnp.float32)
    summed = lax.psum_scatter(
        partial_value.astype(jnp.bfloat16), "tp", scatter_dimension=1, tiled=True
    )
    returned = lax.all_to_all(
        summed.reshape(experts, capacity, summed.shape[1]),
        "ep",
        split_axis=0,
        concat_axis=0,
        tiled=True,
    )
    results = returned.reshape(experts * capacity, summed.shape[1]).astype(jnp.float32)
    mixing = jnp.sum(mix_weights[:, :, None] * by_choice.astype(jnp.float32), axis=1)
    mixed = jnp.dot(mixing, results, precision=lax.Precision.HIGHEST)
    squares = jnp.sum(mixed * mixed, axis=1)
    total = lax.psum(squares, "tp")
    scale = lax.rsqrt(total / width + epsilon)
    return (mixed * scale[:, None] * post_gain).astype(jnp.bfloat16)


def solution(mesh):
    in_specs = (
        P("ep", None),
        P("ep", None),
        P("ep", None),
        P(),
        P("ep", None, "tp"),
        P("ep", None, "tp"),
        P("ep", "tp", None),
        P("tp"),
    )
    out_specs = P("ep", "tp")
    return jax.shard_map(
        on_device, mesh=mesh, in_specs=in_specs, out_specs=out_specs, check_vma=False
    )
```

profile of v0, /device:TPU:0, one launch (start us, length us, event | category | flops | bytes accessed | tf_op | source)
XLA Modules:
  0.0 118.9 jit_solution(7595916630309548866)
XLA Ops:
  6.5 0.0 all-gather.2.cloned.1.call-start
  6.5 0.8 copy.21
  7.3 0.1 eq.29
  7.4 0.1 fusion.26
  7.5 0.2 reduce_window_sum.11
  7.7 0.2 select_reduce_fusion.1
  7.8 0.1 reduce_sum.39
  8.0 0.1 copy.22
  8.0 0.7 multiply_add_fusion
  8.7 0.1 fusion.25
  8.8 1.1 fusion.13
  10.0 1.6 %convolution_convert_fusion.1 = bf16[192,4096]{1,0:T(8,128)(2,1)S(1)} fusion(pred[32,192]{1,0:T(8,128)(4,1)S(1)} %fusion.25, bf16[32,4096]{1,0:T(8,128)(2,1)} %param.8, f32[4096]{0:T(1024)} %param.11, f32[32]{0:T(128)S(1)} %add_rsqrt_fusion.1), kind=kOutput, calls=%fused_computation.1 | convolution fusion | flops 51642368 | bytes 1857664 | tf_op jit(solution)/shard_map/tc,td->cd/dot_general | solution.py:28
  11.6 19.2 %all_to_all.10 = bf16[8,24,1024]{2,1,0:T(8,128)(2,1)} all-to-all(bf16[8,24,1024]{2,1,0:T(8,128)(2,1)S(1)} %constant_dynamic-slice_fusion), channel_id=1, replica_groups=mesh['ep'=8,'tp'=4] {'ep'}, dimensions={0} | all-to-all | bytes 786432 | tf_op jit(solution)/shard_map/all_to_all | solution.py:36
  30.8 0.0 all-gather.2.cloned.1.call-update
  30.9 0.0 reduce-scatter.2.cloned.1.call-start
  30.9 18.4 %all-gather.2.cloned.1.call-done = bf16[8,24,4096]{2,1,0:T(8,128)(2,1)} async-done(((bf16[8,24,1024]{2,1,0:T(8,128)(2,1)}), bf16[8,24,4096]{2,1,0:T(8,128)(2,1)}) %all-gather.2.cloned.1.call-update) | async-done | bytes 1572880 | tf_op jit(solution)/shard_map/all_gather | solution.py:37
  49.4 0.0 copy-start
  49.4 3.7 %fusion.3 = f32[192,512]{1,0:T(8,128)S(1)} fusion(bf16[192,4096]{1,0:T(8,128)(2,1)} %bitcast.26, bf16[1,4096,512]{2,1,0:T(8,128)(2,1)} %param.12), kind=kOutput, calls=%fused_computation.5 | convolution fusion | flops 805306368 | bytes 6160384 | tf_op jit(solution)/shard_map/dot_general | solution.py:39
  53.1 0.0 copy-done
  53.1 0.0 copy-start.2
  53.1 0.0 copy-start.1
  53.1 6.6 %convolution_convert_fusion = bf16[192,4096]{1,0:T(8,128)(2,1)} fusion(bf16[1,512,4096]{2,1,0:T(8,128)(2,1)} %param.14, bf16[192,4096]{1,0:T(8,128)(2,1)S(1)} %bitcast.27, bf16[1,4096,512]{2,1,0:T(8,128)(2,1)} %param.13, f32[192,512]{1,0:T(8,128)S(1)} %fusion.3), kind=kOutput, calls=%fused_computation | convolution fusion | flops 1611988992 | bytes 11927552 | tf_op jit(solution)/shard_map/dot_general | solution.py:42
  59.8 0.0 reduce-scatter.2.cloned.1.call-update
  59.8 28.1 %reduce-scatter.2.cloned.1.call-done = bf16[192,1024]{1,0:T(8,128)(2,1)} async-done(((bf16[192,4096]{1,0:T(8,128)(2,1)}), bf16[192,1024]{1,0:T(8,128)(2,1)}) %reduce-scatter.2.cloned.1.call-update) | async-done | bytes 393232 | tf_op jit(solution)/shard_map/reduce_scatter | solution.py:43
  87.9 5.5 %all-to-all-start.1 = ((bf16[8,24,1024]{2,1,0:T(8,128)(2,1)}), bf16[8,24,1024]{2,1,0:T(8,128)(2,1)S(1)}, u32[]{:S(2)}, u32[]{:S(2)}) async-start(bf16[8,24,1024]{2,1,0:T(8,128)(2,1)} %bitcast.28), calls=%async_computation.2 | async-start | bytes 786432 | tf_op jit(solution)/shard_map/all_to_all | solution.py:46
  93.4 0.0 copy-done.2
  93.4 0.1 select_reduce_fusion
  93.5 11.5 %all-to-all-done.1 = bf16[8,24,1024]{2,1,0:T(8,128)(2,1)S(1)} async-done(((bf16[8,24,1024]{2,1,0:T(8,128)(2,1)}), bf16[8,24,1024]{2,1,0:T(8,128)(2,1)S(1)}, u32[]{:S(2)}, u32[]{:S(2)}) %all-to-all-start.1) | async-done | bytes 393248 | tf_op jit(solution)/shard_map/all_to_all | solution.py:46
  105.0 0.4 multiply_reduce_fusion
  105.4 5.9 %psum.7 = f32[32]{0:T(128)S(1)} all-reduce(f32[32]{0:T(128)S(1)} %get-tuple-element.5), channel_id=1, replica_groups=mesh['ep'=8,'tp'=4] {'tp'}, use_global_device_ids=true, to_apply=%region_7.8 | all-reduce | flops 32 | bytes 256 | tf_op jit(solution)/shard_map/psum | solution.py:57
  111.3 0.0 copy-done.1
  111.3 0.7 multiply_convert_fusion
  (3 shorter events, 0.1 us)
Async XLA Ops:
  6.5 42.8 %all-gather.2.cloned.1.call-start = ((), (), s32[]{:S(2)}) async-start(), calls=%async_computation.3 | async-start | bytes 1966080 | tf_op jit(solution)/shard_map/all_gather | solution.py:37
  30.9 57.1 %reduce-scatter.2.cloned.1.call-start = ((), (), s32[]{:S(2)}) async-start(), calls=%async_computation.4 | async-start | bytes 1966080 | tf_op jit(solution)/shard_map/reduce_scatter | solution.py:43
  49.4 3.8 %copy-start = (bf16[8,24,4096]{2,1,0:T(8,128)(2,1)S(1)}, bf16[8,24,4096]{2,1,0:T(8,128)(2,1)}, u32[]{:S(2)}) copy-start(bf16[8,24,4096]{2,1,0:T(8,128)(2,1)} %all-gather.2.cloned.1.call-done) | copy-start | bytes 4718596
  53.1 40.3 %copy-start.2 = (f32[32,4]{0,1:T(4,128)S(1)}, f32[32,4]{0,1:T(4,128)}, u32[]{:S(2)}) copy-start(f32[32,4]{0,1:T(4,128)} %param.10) | copy-start | bytes 1540
  53.1 58.2 %copy-start.1 = (f32[1024]{0:T(1024)S(1)}, f32[1024]{0:T(1024)}, u32[]{:S(2)}) copy-start(f32[1024]{0:T(1024)} %param.15) | copy-start | bytes 12292
  87.9 17.1 %all-to-all-start.1 = ((bf16[8,24,1024]{2,1,0:T(8,128)(2,1)}), bf16[8,24,1024]{2,1,0:T(8,128)(2,1)S(1)}, u32[]{:S(2)}, u32[]{:S(2)}) async-start(bf16[8,24,1024]{2,1,0:T(8,128)(2,1)} %bitcast.28), calls=%async_computation.2 | async-start | bytes 786432 | tf_op jit(solution)/shard_map/all_to_all | solution.py:46
Sparse Core Ops, SparseCore 0:
  31.0 18.3 all-gather.1
  59.9 27.9 reduce-scatter.1
where the time goes:
time: 119 us
  waiting for transfers between devices  58.1 us (49%)
  blocking collectives  25.2 us (21%)
  between operations  13.5 us (11%)
  matrix products  12.3 us (10%)
  starting transfers between devices  5.53 us (5%)
  other arithmetic  3.16 us (3%)
    reduce_scatter x1, waiting for transfers between devices, on_device(): lax.psum_scatter(partial_value.astype(jnp.bfloat16), 'tp', scatter_dimens...  28.1 us
    all_to_all x1, blocking collectives, on_device(): lax.all_to_all(outgoing_part, 'ep', split_axis=0, concat_axis=0, tiled=True)  19.2 us
    all_gather x1, waiting for transfers between devices, on_device(): arrived = lax.all_gather(arrived, 'tp', axis=2, tiled=True)  18.4 us
    all_to_all x1, waiting for transfers between devices, on_device(): lax.all_to_all(summed.reshape(experts, capacity, summed.shape[1]), 'ep',...  11.5 us
    dot_general x1, matrix products, on_device(): jnp.dot(hidden, down_weight[0], preferred_element_type=jnp.float32)  6.61 us
    psum x1, blocking collectives, on_device(): total = lax.psum(squares, 'tp')  5.95 us
    all_to_all x1, starting transfers between devices, on_device(): lax.all_to_all(summed.reshape(experts, capacity, summed.shape[1]), 'ep',...  5.48 us
    dot_general x1, matrix products, on_device(): jnp.dot(arrived_rows, gate_weight[0], preferred_element_type=jnp.float32)  3.75 us
  transfers between devices with their start and end apart: 3, of which 3 were waited for; matrix products, arithmetic and copies ran while one was open for 0% of the time, Pallas kernels for 0%

commit v1 on v0

--- a/solution.py
+++ b/solution.py
@@ -34,7 +34,12 @@
         outgoing, lax.axis_index("tp") * slice_width, slice_width, 2
     )
     arrived = lax.all_to_all(outgoing_part, "ep", split_axis=0, concat_axis=0, tiled=True)
-    arrived = lax.all_gather(arrived, "tp", axis=2, tiled=True)
+    ring = [arrived]
+    for hop in range(3):
+        ring.append(lax.ppermute(ring[-1], "tp", [(dev, (dev + 1) % 4) for dev in range(4)]))
+    arrived = jnp.roll(
+        jnp.concatenate(ring[::-1], axis=2), (lax.axis_index("tp") + 1) * ring[0].shape[2], axis=2
+    )
     arrived_rows = arrived.reshape(experts * capacity, width)
     gate_act = jnp.dot(arrived_rows, gate_weight[0], preferred_element_type=jnp.float32)
     up_act = jnp.dot(arrived_rows, up_weight[0], preferred_element_type=jnp.float32)

time: 119 us -> 121 us (1.017)
  matrix products: 12.3 us -> 9.61 us
  local copies, waits for them, and re-layouts: 1.1 us -> 3.35 us
  waiting for transfers between devices: 58.1 us -> 60 us
    ppermute x0 -> x3, waiting for transfers between devices: none -> 21.6 us  [on_device(): lax.ppermute(ring[-1], 'tp', [(dev, (dev + 1) % 4) for dev in range(4)])]
    all_gather x1 -> x0, waiting for transfers between devices: 18.4 us -> none  [on_device(): arrived = lax.all_gather(arrived, 'tp', axis=2, tiled=True)]
    dot_general x1, matrix products: 3.75 us -> 1.01 us  [on_device(): jnp.dot(arrived_rows, gate_weight[0], preferred_element_type=jnp.float32)]
    unnamed x7 -> x14, local copies, waits for them, and re-layouts: 0.78 us -> 2.85 us
    reduce_scatter x1, waiting for transfers between devices: 28.1 us -> 26.9 us  [on_device(): lax.psum_scatter(partial_value.astype(jnp.bfloat16), 'tp', scatter_dimens...]
  transfers between devices with their start and end apart: 3 -> 5, of which waited for: 3 -> 5; matrix products, arithmetic and copies ran while one was open for 0% -> 0% of each run, Pallas kernels for 0% -> 0%
where the time goes in v1:
time: 121 us; the launch traced here: 120 us
  waiting for transfers between devices  60 us (50%)
  blocking collectives  25.1 us (21%)
  between operations  13.6 us (11%)
  matrix products  9.61 us (8%)
  starting transfers between devices  5.52 us (5%)
  local copies, waits for them, and re-layouts  3.35 us (3%)
  other arithmetic  3.16 us (3%)
    reduce_scatter x1, waiting for transfers between devices, on_device(): lax.psum_scatter(partial_value.astype(jnp.bfloat16), 'tp', scatter_dimens...  26.9 us
    ppermute x3, waiting for transfers between devices, on_device(): lax.ppermute(ring[-1], 'tp', [(dev, (dev + 1) % 4) for dev in range(4)])  21.6 us
    all_to_all x1, blocking collectives, on_device(): lax.all_to_all(outgoing_part, 'ep', split_axis=0, concat_axis=0, tiled=True)  19.1 us
    all_to_all x1, waiting for transfers between devices, on_device(): lax.all_to_all(summed.reshape(experts, capacity, summed.shape[1]), 'ep',...  11.4 us
    dot_general x1, matrix products, on_device(): jnp.dot(hidden, down_weight[0], preferred_element_type=jnp.float32)  6.61 us
    psum x1, blocking collectives, on_device(): total = lax.psum(squares, 'tp')  5.95 us
    all_to_all x1, starting transfers between devices, on_device(): lax.all_to_all(summed.reshape(experts, capacity, summed.shape[1]), 'ep',...  5.51 us
    unnamed x14, local copies, waits for them, and re-layouts  2.85 us
  transfers between devices with their start and end apart: 5, of which 5 were waited for; matrix products, arithmetic and copies ran while one was open for 0% of the time, Pallas kernels for 0%

profile of v1, /device:TPU:0, one launch (start us, length us, event | category | flops | bytes accessed | tf_op | source)
XLA Modules:
  0.0 120.2 jit_solution(13001875478415825507)
XLA Ops:
  6.5 0.0 reduce-scatter.2.cloned.1.call-start
  6.5 0.8 copy.21
  7.3 0.1 eq.32
  7.4 0.1 fusion.26
  7.5 0.2 reduce_window_sum.11
  7.7 0.2 select_reduce_fusion.1
  7.8 0.1 reduce_sum.39
  8.0 0.1 copy.22
  8.0 0.7 multiply_add_fusion
  8.7 0.1 fusion.25
  8.8 1.1 fusion.13
  10.0 1.6 %convolution_convert_fusion.1 = bf16[192,4096]{1,0:T(8,128)(2,1)S(1)} fusion(pred[32,192]{1,0:T(8,128)(4,1)S(1)} %fusion.25, bf16[32,4096]{1,0:T(8,128)(2,1)} %param.8, f32[4096]{0:T(1024)} %param.11, f32[32]{0:T(128)S(1)} %add_rsqrt_fusion.1), kind=kOutput, calls=%fused_computation.1 | convolution fusion | flops 51642368 | bytes 1857664 | tf_op jit(solution)/shard_map/tc,td->cd/dot_general | solution.py:28
  11.6 19.1 %all_to_all.10 = bf16[8,24,1024]{2,1,0:T(8,128)(2,1)S(1)} all-to-all(bf16[8,24,1024]{2,1,0:T(8,128)(2,1)S(1)} %constant_dynamic-slice_fusion), channel_id=1, replica_groups=mesh['ep'=8,'tp'=4] {'ep'}, dimensions={0} | all-to-all | bytes 786432 | tf_op jit(solution)/shard_map/all_to_all | solution.py:36
  30.7 0.0 collective-permute-start
  30.7 7.2 %collective-permute-done = bf16[8,24,1024]{2,1,0:T(8,128)(2,1)S(1)} collective-permute-done((bf16[8,24,1024]{2,1,0:T(8,128)(2,1)S(1)}, bf16[8,24,1024]{2,1,0:T(8,128)(2,1)S(1)}, u32[]{:S(2)}, u32[]{:S(2)}) %collective-permute-start) | collective-permute-done | bytes 393248 | tf_op jit(solution)/shard_map/ppermute | solution.py:39
  37.9 0.0 collective-permute-start.1
  37.9 7.2 %collective-permute-done.1 = bf16[8,24,1024]{2,1,0:T(8,128)(2,1)S(1)} collective-permute-done((bf16[8,24,1024]{2,1,0:T(8,128)(2,1)S(1)}, bf16[8,24,1024]{2,1,0:T(8,128)(2,1)S(1)}, u32[]{:S(2)}, u32[]{:S(2)}) %collective-permute-start.1) | collective-permute-done | bytes 393248 | tf_op jit(solution)/shard_map/ppermute | solution.py:39
  45.1 0.0 collective-permute-start.2
  45.1 7.2 %collective-permute-done.2 = bf16[8,24,1024]{2,1,0:T(8,128)(2,1)S(1)} collective-permute-done((bf16[8,24,1024]{2,1,0:T(8,128)(2,1)S(1)}, bf16[8,24,1024]{2,1,0:T(8,128)(2,1)S(1)}, u32[]{:S(2)}, u32[]{:S(2)}) %collective-permute-start.2) | collective-permute-done | bytes 393248 | tf_op jit(solution)/shard_map/ppermute | solution.py:39
  52.5 0.0 copy-start
  52.6 0.2 constant_dynamic-slice_fusion.1
  52.8 1.9 %copy-done = bf16[1,4096,512]{2,1,0:T(8,128)(2,1)S(1)} copy-done((bf16[1,4096,512]{2,1,0:T(8,128)(2,1)S(1)}, bf16[1,4096,512]{2,1,0:T(8,128)(2,1)}, u32[]{:S(2)}) %copy-start) | copy-done | bytes 4194328
  54.7 1.0 fusion.3
  55.7 0.0 copy-start.2
  55.7 0.0 copy-start.1
  55.7 6.6 %convolution_convert_fusion = bf16[192,4096]{1,0:T(8,128)(2,1)} fusion(bf16[1,512,4096]{2,1,0:T(8,128)(2,1)} %param.14, bf16[192,4096]{1,0:T(8,128)(2,1)S(1)} %bitcast.25, bf16[1,4096,512]{2,1,0:T(8,128)(2,1)} %param.13, f32[192,512]{1,0:T(8,128)S(1)} %fusion.3), kind=kOutput, calls=%fused_computation | convolution fusion | flops 1611988992 | bytes 11927552 | tf_op jit(solution)/shard_map/dot_general | solution.py:47
  62.3 0.0 reduce-scatter.2.cloned.1.call-update
  62.3 26.9 %reduce-scatter.2.cloned.1.call-done = bf16[192,1024]{1,0:T(8,128)(2,1)} async-done(((bf16[192,4096]{1,0:T(8,128)(2,1)}), bf16[192,1024]{1,0:T(8,128)(2,1)}) %reduce-scatter.2.cloned.1.call-update) | async-done | bytes 393232 | tf_op jit(solution)/shard_map/reduce_scatter | solution.py:48
  89.3 5.5 %all-to-all-start.1 = ((bf16[8,24,1024]{2,1,0:T(8,128)(2,1)}), bf16[8,24,1024]{2,1,0:T(8,128)(2,1)S(1)}, u32[]{:S(2)}, u32[]{:S(2)}) async-start(bf16[8,24,1024]{2,1,0:T(8,128)(2,1)} %bitcast.28), calls=%async_computation.2 | async-start | bytes 786432 | tf_op jit(solution)/shard_map/all_to_all | solution.py:51
  94.8 0.0 copy-done.2
  94.8 0.1 select_reduce_fusion
  94.9 11.4 %all-to-all-done.1 = bf16[8,24,1024]{2,1,0:T(8,128)(2,1)S(1)} async-done(((bf16[8,24,1024]{2,1,0:T(8,128)(2,1)}), bf16[8,24,1024]{2,1,0:T(8,128)(2,1)S(1)}, u32[]{:S(2)}, u32[]{:S(2)}) %all-to-all-start.1) | async-done | bytes 393248 | tf_op jit(solution)/shard_map/all_to_all | solution.py:51
  106.3 0.4 multiply_reduce_fusion
  106.7 6.0 %psum.7 = f32[32]{0:T(128)S(1)} all-reduce(f32[32]{0:T(128)S(1)} %get-tuple-element.5), channel_id=1, replica_groups=mesh['ep'=8,'tp'=4] {'tp'}, use_global_device_ids=true, to_apply=%region_7.8 | all-reduce | flops 32 | bytes 256 | tf_op jit(solution)/shard_map/psum | solution.py:62
  112.7 0.0 copy-done.1
  112.7 0.7 multiply_convert_fusion
  (11 shorter events, 0.3 us)
Async XLA Ops:
  6.5 82.7 %reduce-scatter.2.cloned.1.call-start = ((), (), s32[]{:S(2)}) async-start(), calls=%async_computation.3 | async-start | bytes 1966080 | tf_op jit(solution)/shard_map/reduce_scatter | solution.py:48
  30.7 7.2 %collective-permute-start = (bf16[8,24,1024]{2,1,0:T(8,128)(2,1)S(1)}, bf16[8,24,1024]{2,1,0:T(8,128)(2,1)S(1)}, u32[]{:S(2)}, u32[]{:S(2)}) collective-permute-start(bf16[8,24,1024]{2,1,0:T(8,128)(2,1)S(1)} %all_to_all.10), channel_id=1, source_target_pairs={{0,1},{1,2},{2,3},{3,0},{4,5},{5,6},{6,7},{7,4},{8,9},{9,10},{10,1... | collective-permute-start | bytes 1179656 | tf_op jit(solution)/shard_map/ppermute | solution.py:39
  37.9 7.2 %collective-permute-start.1 = (bf16[8,24,1024]{2,1,0:T(8,128)(2,1)S(1)}, bf16[8,24,1024]{2,1,0:T(8,128)(2,1)S(1)}, u32[]{:S(2)}, u32[]{:S(2)}) collective-permute-start(bf16[8,24,1024]{2,1,0:T(8,128)(2,1)S(1)} %collective-permute-done), channel_id=1, source_target_pairs={{0,1},{1,2},{2,3},{3,0},{4,5},{5,6},{6,7},{7,4},{8,9},{9,10},{10,1... | collective-permute-start | bytes 1179656 | tf_op jit(solution)/shard_map/ppermute | solution.py:39
  45.1 7.2 %collective-permute-start.2 = (bf16[8,24,1024]{2,1,0:T(8,128)(2,1)S(1)}, bf16[8,24,1024]{2,1,0:T(8,128)(2,1)S(1)}, u32[]{:S(2)}, u32[]{:S(2)}) collective-permute-start(bf16[8,24,1024]{2,1,0:T(8,128)(2,1)S(1)} %collective-permute-done.1), channel_id=1, source_target_pairs={{0,1},{1,2},{2,3},{3,0},{4,5},{5,6},{6,7},{7,4},{8,9},{9,10},{10,1... | collective-permute-start | bytes 1179656 | tf_op jit(solution)/shard_map/ppermute | solution.py:39
  52.5 2.2 %copy-start = (bf16[1,4096,512]{2,1,0:T(8,128)(2,1)S(1)}, bf16[1,4096,512]{2,1,0:T(8,128)(2,1)}, u32[]{:S(2)}) copy-start(bf16[1,4096,512]{2,1,0:T(8,128)(2,1)} %param.12) | copy-start | bytes 12582916
  55.7 39.1 %copy-start.2 = (f32[32,4]{0,1:T(4,128)S(1)}, f32[32,4]{0,1:T(4,128)}, u32[]{:S(2)}) copy-start(f32[32,4]{0,1:T(4,128)} %param.10) | copy-start | bytes 1540
  55.7 57.0 %copy-start.1 = (f32[1024]{0:T(1024)S(1)}, f32[1024]{0:T(1024)}, u32[]{:S(2)}) copy-start(f32[1024]{0:T(1024)} %param.15) | copy-start | bytes 12292
  89.3 17.1 %all-to-all-start.1 = ((bf16[8,24,1024]{2,1,0:T(8,128)(2,1)}), bf16[8,24,1024]{2,1,0:T(8,128)(2,1)S(1)}, u32[]{:S(2)}, u32[]{:S(2)}) async-start(bf16[8,24,1024]{2,1,0:T(8,128)(2,1)} %bitcast.28), calls=%async_computation.2 | async-start | bytes 786432 | tf_op jit(solution)/shard_map/all_to_all | solution.py:51
Sparse Core Ops, SparseCore 0:
  62.5 26.7 reduce-scatter.1
